TPU v7x, 32 devices: a whole 2x2x4 slice. The times are simulated.
32 devices in a mesh: sp: 8 (over z, y), tp: 4 (over x, core).
Axes of the slice: x: 2, y: 2, z: 4, core: 2. Of those that a mesh axis runs over, the one named last changes fastest.
Arguments:
- latents: bfloat16 [2048, 4096], P('sp'), may hold values from -0.4375 to 0.4375
- query_heads: bfloat16 [2048, 16, 128], P('sp', 'tp'), may hold values from -8 to 8
- key_heads: bfloat16 [2048, 16, 128], P('sp', 'tp'), may hold values from -8 to 8
- value_heads: bfloat16 [2048, 16, 128], P('sp', 'tp'), may hold values from -6 to 6
- map_outputs: bfloat16 [2048, 2, 16, 128], P('sp', None, 'tp'), may hold values from -6 to 6
- log_sums: float32 [2048, 16, 2], P('sp', 'tp'), may hold values from -600 to 600, as said below
- out_grad: bfloat16 [2048, 16, 128], P('sp', 'tp'), may hold values from -6 to 6
- mix_lambda: float32 [16], P('tp'), may hold values from 0.3 to 0.8
- norm_gain: float32 [128], replicated, may hold values from 0.1 to 1.9
Outputs:
- query_grad: bfloat16 [2048, 16, 128], P('sp', 'tp')
- key_grad: bfloat16 [2048, 16, 128], P('sp', 'tp')
- value_grad: bfloat16 [2048, 16, 128], P('sp', 'tp')
- weight_grad: float32 [4096, 2048], P('sp', 'tp')
Inputs may be any that keep to these rules, and one draw needn't show every extreme that they name: query_heads, key_heads and value_heads together with map_outputs and log_sums are one consistent causal forward pass: log_sums is the row's log-sum of exp(score_m) over keys at or before the row, and map_outputs[:, m] is prob_m times value_heads rounded to bfloat16.
All inputs are finite; a program needn't handle non-finite values.
Results may differ from a plain program's by a relative error of at most 0.019.
Values may be sent and summed in bfloat16 or wider, within the bound.
A program may use at most 64 MiB of HBM per device.

v0:
```python
import jax
import jax.numpy as jnp
from jax import lax
from jax.sharding import PartitionSpec as P

DH = 64
EPSILON = 1e-05


def norm_backward(map_outputs, out_grad, mix_lambda, norm_gain):
    first_map = map_outputs[:, 0].astype(jnp.float32)
    second_map = map_outputs[:, 1].astype(jnp.float32)
    lambda_col = mix_lambda[None, :, None]
    combined = first_map - lambda_col * second_map
    inverse = lax.rsqrt(jnp.mean(combined * combined, axis=-1, keepdims=True) + EPSILON)
    weighted = norm_gain[None, None, :] * out_grad.astype(jnp.float32)
    grad_out = (
        inverse * weighted
        - inverse**3 * combined * jnp.mean(combined * weighted, axis=-1, keepdims=True)
    ).astype(jnp.bfloat16)
    grad_wide = grad_out.astype(jnp.float32)
    row_terms = jnp.stack(
        [jnp.sum(grad_wide * first_map, axis=-1), jnp.sum(grad_wide * second_map, axis=-1)], axis=-1
    )
    return (grad_out, row_terms)


def block_grads(
    query_blk, grad_blk, lse_blk, term_blk, key_blk, value_blk, query_pos, key_pos, mix_lambda
):
    row_count = query_blk.shape[0]
    col_count = key_blk.shape[0]
    head_count = query_blk.shape[1]
    score_scale = DH ** (-0.5)
    query_split = query_blk.reshape(row_count, head_count, 2, DH)
    key_split = key_blk.reshape(col_count, head_count, 2, DH)
    scores = (
        jnp.einsum("qhmd,khmd->hmqk", query_split, key_split, preferred_element_type=jnp.float32)
        * score_scale
    )
    causal = key_pos[None, :] <= query_pos[:, None]
    softmax_maps = jnp.exp(
        jnp.where(causal, scores - jnp.transpose(lse_blk, (1, 2, 0))[..., None], -jnp.inf)
    )
    mixed_grad = jnp.einsum("qhe,khe->hqk", grad_blk, value_blk, preferred_element_type=jnp.float32)
    map_signs = jnp.stack([jnp.ones_like(mix_lambda), -mix_lambda], axis=1)[:, :, None, None]
    score_grad = (
        map_signs
        * softmax_maps
        * (mixed_grad[:, None] - jnp.transpose(term_blk, (1, 2, 0))[..., None])
    ).astype(jnp.bfloat16)
    diff_weights = (softmax_maps[:, 0] - mix_lambda[:, None, None] * softmax_maps[:, 1]).astype(
        jnp.bfloat16
    )
    value_part = jnp.einsum(
        "hqk,qhe->khe", diff_weights, grad_blk, preferred_element_type=jnp.float32
    )
    query_part = score_scale * jnp.einsum(
        "hmqk,khmd->qhmd", score_grad, key_split, preferred_element_type=jnp.float32
    )
    key_part = score_scale * jnp.einsum(
        "hmqk,qhmd->khmd", score_grad, query_split, preferred_element_type=jnp.float32
    )
    return (
        query_part.reshape(row_count, head_count, 2 * DH),
        key_part.reshape(col_count, head_count, 2 * DH),
        value_part,
    )


def unchanged(running):
    return running


def body(
    latents,
    query_heads,
    key_heads,
    value_heads,
    map_outputs,
    log_sums,
    out_grad,
    mix_lambda,
    norm_gain,
):
    rows_dev = query_heads.shape[0]
    head_count = query_heads.shape[1]
    width = query_heads.shape[2]
    offset = lax.axis_index("sp") * rows_dev
    own_pos = offset + jnp.arange(rows_dev, dtype=jnp.int32)
    grad_out, row_terms = norm_backward(map_outputs, out_grad, mix_lambda, norm_gain)
    local_zero = jnp.zeros((rows_dev, head_count, width), jnp.float32)
    row_stats = jnp.concatenate([log_sums, row_terms], axis=-1)
    all_stats = lax.all_gather(row_stats, "sp", axis=0, tiled=True)
    key_piece = lax.all_gather(key_heads, "sp", axis=0, tiled=True)
    value_piece = lax.all_gather(value_heads, "sp", axis=0, tiled=True)
    pieces = key_piece.shape[0] // rows_dev
    blocks = (
        key_piece.reshape(pieces, rows_dev, head_count, width),
        value_piece.reshape(pieces, rows_dev, head_count, width),
        jnp.arange(pieces, dtype=jnp.int32),
    )

    def visit(state, element):
        key_blk, value_blk, block_index = element
        first_key = block_index * rows_dev

        def accumulate(query_acc):
            key_pos = first_key + jnp.arange(rows_dev, dtype=jnp.int32)
            query_part, _, _ = block_grads(
                query_heads,
                grad_out,
                log_sums,
                row_terms,
                key_blk,
                value_blk,
                own_pos,
                key_pos,
                mix_lambda,
            )
            return query_acc + query_part

        return (lax.cond(first_key < offset + rows_dev, accumulate, unchanged, state), None)

    result, _ = lax.scan(visit, local_zero, blocks)
    query_acc = result
    query_piece = lax.all_gather(query_heads, "sp", axis=0, tiled=True)
    grad_piece = lax.all_gather(grad_out, "sp", axis=0, tiled=True)
    pieces = query_piece.shape[0] // rows_dev
    blocks = (
        query_piece.reshape(pieces, rows_dev, head_count, width),
        grad_piece.reshape(pieces, rows_dev, head_count, width),
        jnp.arange(pieces, dtype=jnp.int32),
    )

    def visit(state, element):
        query_blk, grad_blk, block_index = element
        first_query = block_index * rows_dev

        def accumulate(inner):
            key_acc, value_acc = inner
            query_pos = first_query + jnp.arange(rows_dev, dtype=jnp.int32)
            stats_blk = lax.dynamic_slice_in_dim(all_stats, first_query, rows_dev, 0)
            _, key_part, value_part = block_grads(
                query_blk,
                grad_blk,
                stats_blk[..., :2],
                stats_blk[..., 2:],
                key_heads,
                value_heads,
                query_pos,
                own_pos,
                mix_lambda,
            )
            return (key_acc + key_part, value_acc + value_part)

        return (lax.cond(first_query + rows_dev > offset, accumulate, unchanged, state), None)

    result, _ = lax.scan(visit, (local_zero, local_zero), blocks)
    key_acc, value_acc = result
    query_grad = query_acc.astype(jnp.bfloat16)
    flat_grad = query_grad.reshape(rows_dev, head_count * width)
    weight_grad = lax.psum_scatter(
        lax.dot_general(
            latents, flat_grad, (((0,), (0,)), ((), ())), preferred_element_type=jnp.float32
        ).astype(jnp.bfloat16),
        "sp",
        scatter_dimension=0,
        tiled=True,
    ).astype(jnp.float32)
    return (query_grad, key_acc.astype(jnp.bfloat16), value_acc.astype(jnp.bfloat16), weight_grad)


def solution(mesh):
    placed = (
        P("sp", None),
        P("sp", "tp", None),
        P("sp", "tp", None),
        P("sp", "tp", None),
        P("sp", None, "tp", None),
        P("sp", "tp", None),
        P("sp", "tp", None),
        P("tp"),
        P(),
    )
    return jax.shard_map(
        body,
        mesh=mesh,
        in_specs=placed,
        out_specs=(P("sp", "tp", None), P("sp", "tp", None), P("sp", "tp", None), P("sp", "tp")),
        check_vma=False,
    )
```

profile of v0, /device:TPU:0, one launch (start us, length us, event | category | flops | bytes accessed | tf_op | source)
XLA Modules:
  0.0 374.7 jit_solution(14575236369134222766)
XLA Ops:
  15.9 46.7 %all-gather.5.cloned.1.call-done = bf16[2048,4,128]{2,0,1:T(8,128)(2,1)} async-done(((bf16[256,4,128]{2,0,1:T(8,128)(2,1)}), bf16[2048,4,128]{2,0,1:T(8,128)(2,1)}) %all-gather.5.cloned.1.call-update) | async-done | bytes 2097168 | tf_op jit(solution)/shard_map/all_gather | solution.py:95
  62.6 3.9 %copy.54 = bf16[8,256,4,128]{1,3,2,0:T(8,128)(2,1)} copy(bf16[8,256,4,128]{3,1,0,2:T(8,128)(2,1)} %bitcast.124) | data formatting | bytes 4194304
  66.5 45.8 %all-gather.7.cloned.1.call-done = bf16[2048,4,128]{2,1,0:T(4,128)(2,1)} async-done(((bf16[256,4,128]{2,1,0:T(4,128)(2,1)}), bf16[2048,4,128]{2,1,0:T(4,128)(2,1)}) %all-gather.7.cloned.1.call-update) | async-done | bytes 2097168 | tf_op jit(solution)/shard_map/all_gather | solution.py:96
  112.4 3.5 copy.56
  116.7 19.2 %while.30 = (s32[]{:T(128)}, f32[256,4,128]{0,2,1:T(8,128)}, s32[8]{0:T(128)S(1)}, s32[]{:T(128)}, f32[4]{0:T(128)}, /*index=5*/bf16[8,256,4,128]{1,3,2,0:T(8,12...) while((s32[]{:T(128)}, f32[256,4,128]{0,2,1:T(8,128)}, ...), condition=%wide.region_7.8_spmd.clone, body=%wide.region_4.7_spmd.clone.sunk | while | flops 205324800 | bytes 5921723 | solution.py:125
  118.0 8.9 %conditional.7 = (f32[256,4,128]{0,2,1:T(8,128)}) conditional(s32[]{:T(128)} %convert_element_type.109, f32[256,4,128]{0,2,1:T(8,128)} %get-tuple-element.780, (f32[4]{0:T(128)}, s32[]{:T(128)}, s32[]{:T(128)}, bf16[8,256,4,128]{1,3,2,0:T(8,128)(2,1)}, s32[]{:T(128)}, /*index=5*/bf16[256,4,128]{0,2,1:T(8,128)(2,1)}, f32[256,4,2]{0,2,1:T(2,128)S(1)}, ...), branch_computations={%region_5.5_spmd, %region_6.6_spmd} | conditional | flops 205324800 | bytes 5920424 | solution.py:123
  121.9 3.0 fusion.9
  137.2 3.2 fusion.38
  143.0 90.8 %all_gather.18 = f32[2048,4,4]{0,2,1:T(4,128)S(1)} all-gather(f32[256,4,4]{0,2,1:T(4,128)S(1)} %pad_maximum_fusion), channel_id=1, replica_groups=mesh['sp'=8,'tp'=4] {'sp'}, dimensions={0}, use_global_device_ids=true | all-gather | bytes 147456 | tf_op jit(solution)/shard_map/all_gather | solution.py:94
  233.9 4.0 %copy.60 = bf16[8,256,4,128]{1,3,2,0:T(8,128)(2,1)} copy(bf16[8,256,4,128]{3,1,0,2:T(8,128)(2,1)} %bitcast.122) | data formatting | bytes 4194304
  237.8 3.3 copy.62
  243.3 118.6 %while.31 = (s32[]{:T(128)}, f32[256,4,128]{0,2,1:T(8,128)}, f32[256,4,128]{2,0,1:T(8,128)}, s32[8]{0:T(128)}, s32[]{:T(128)}, /*index=5*/f32[4]{0:T(128)}, bf16...) while((s32[]{:T(128)}, f32[256,4,128]{0,2,1:T(8,128)}, ...), condition=%wide.region_11.12_spmd.clone.clone, body=%wide.region_8.11_spmd.clone.clone.sunk | while | flops 273351168 | bytes 23257172 | solution.py:159
  245.2 12.9 %conditional.8 = ((f32[256,4,128]{0,2,1:T(8,128)}, f32[256,4,128]{2,0,1:T(8,128)})) conditional(s32[]{:T(128)} %convert_element_type.110, (f32[256,4,128]{0,2,1:T(8,128)}, f32[256,4,128]{2,0,1:T(8,128)}) %tuple.101, (f32[4]{0:T(128)}, s32[]{:T(128)}, s32[]{:T(128)}, bf16[8,256,4,128]{1,3,2,0:T(8,128)(2,1)}, s32[]{:T(128)}, ...), branch_computations={%region_9.9_spmd, %region_10.10_spmd} | conditional | flops 273351168 | bytes 23255846 | solution.py:157
  246.5 3.0 select_exponential_fusion
  255.8 2.4 fusion.22
  260.1 12.9 %conditional.8 = ((f32[256,4,128]{0,2,1:T(8,128)}, f32[256,4,128]{2,0,1:T(8,128)})) conditional(s32[]{:T(128)} %convert_element_type.110, (f32[256,4,128]{0,2,1:T(8,128)}, f32[256,4,128]{2,0,1:T(8,128)}) %tuple.101, (f32[4]{0:T(128)}, s32[]{:T(128)}, s32[]{:T(128)}, bf16[8,256,4,128]{1,3,2,0:T(8,128)(2,1)}, s32[]{:T(128)}, ...), branch_computations={%region_9.9_spmd, %region_10.10_spmd} | conditional | flops 273351168 | bytes 23255846 | solution.py:157
  261.3 3.0 select_exponential_fusion
  275.0 12.9 %conditional.8 = ((f32[256,4,128]{0,2,1:T(8,128)}, f32[256,4,128]{2,0,1:T(8,128)})) conditional(s32[]{:T(128)} %convert_element_type.110, (f32[256,4,128]{0,2,1:T(8,128)}, f32[256,4,128]{2,0,1:T(8,128)}) %tuple.101, (f32[4]{0:T(128)}, s32[]{:T(128)}, s32[]{:T(128)}, bf16[8,256,4,128]{1,3,2,0:T(8,128)(2,1)}, s32[]{:T(128)}, ...), branch_computations={%region_9.9_spmd, %region_10.10_spmd} | conditional | flops 273351168 | bytes 23255846 | solution.py:157
  276.2 3.0 select_exponential_fusion
  289.8 12.9 %conditional.8 = ((f32[256,4,128]{0,2,1:T(8,128)}, f32[256,4,128]{2,0,1:T(8,128)})) conditional(s32[]{:T(128)} %convert_element_type.110, (f32[256,4,128]{0,2,1:T(8,128)}, f32[256,4,128]{2,0,1:T(8,128)}) %tuple.101, (f32[4]{0:T(128)}, s32[]{:T(128)}, s32[]{:T(128)}, bf16[8,256,4,128]{1,3,2,0:T(8,128)(2,1)}, s32[]{:T(128)}, ...), branch_computations={%region_9.9_spmd, %region_10.10_spmd} | conditional | flops 273351168 | bytes 23255846 | solution.py:157
  291.0 3.0 select_exponential_fusion
  304.6 12.9 %conditional.8 = ((f32[256,4,128]{0,2,1:T(8,128)}, f32[256,4,128]{2,0,1:T(8,128)})) conditional(s32[]{:T(128)} %convert_element_type.110, (f32[256,4,128]{0,2,1:T(8,128)}, f32[256,4,128]{2,0,1:T(8,128)}) %tuple.101, (f32[4]{0:T(128)}, s32[]{:T(128)}, s32[]{:T(128)}, bf16[8,256,4,128]{1,3,2,0:T(8,128)(2,1)}, s32[]{:T(128)}, ...), branch_computations={%region_9.9_spmd, %region_10.10_spmd} | conditional | flops 273351168 | bytes 23255846 | solution.py:157
  305.9 3.0 select_exponential_fusion
  315.1 2.4 fusion.22
  319.4 12.9 %conditional.8 = ((f32[256,4,128]{0,2,1:T(8,128)}, f32[256,4,128]{2,0,1:T(8,128)})) conditional(s32[]{:T(128)} %convert_element_type.110, (f32[256,4,128]{0,2,1:T(8,128)}, f32[256,4,128]{2,0,1:T(8,128)}) %tuple.101, (f32[4]{0:T(128)}, s32[]{:T(128)}, s32[]{:T(128)}, bf16[8,256,4,128]{1,3,2,0:T(8,128)(2,1)}, s32[]{:T(128)}, ...), branch_computations={%region_9.9_spmd, %region_10.10_spmd} | conditional | flops 273351168 | bytes 23255846 | solution.py:157
  320.7 3.0 select_exponential_fusion
  329.9 2.4 fusion.22
  334.2 12.9 %conditional.8 = ((f32[256,4,128]{0,2,1:T(8,128)}, f32[256,4,128]{2,0,1:T(8,128)})) conditional(s32[]{:T(128)} %convert_element_type.110, (f32[256,4,128]{0,2,1:T(8,128)}, f32[256,4,128]{2,0,1:T(8,128)}) %tuple.101, (f32[4]{0:T(128)}, s32[]{:T(128)}, s32[]{:T(128)}, bf16[8,256,4,128]{1,3,2,0:T(8,128)(2,1)}, s32[]{:T(128)}, ...), branch_computations={%region_9.9_spmd, %region_10.10_spmd} | conditional | flops 273351168 | bytes 23255846 | solution.py:157
  335.5 3.0 select_exponential_fusion
  344.7 2.4 fusion.22
  349.0 12.9 %conditional.8 = ((f32[256,4,128]{0,2,1:T(8,128)}, f32[256,4,128]{2,0,1:T(8,128)})) conditional(s32[]{:T(128)} %convert_element_type.110, (f32[256,4,128]{0,2,1:T(8,128)}, f32[256,4,128]{2,0,1:T(8,128)}) %tuple.101, (f32[4]{0:T(128)}, s32[]{:T(128)}, s32[]{:T(128)}, bf16[8,256,4,128]{1,3,2,0:T(8,128)(2,1)}, s32[]{:T(128)}, ...), branch_computations={%region_9.9_spmd, %region_10.10_spmd} | conditional | flops 273351168 | bytes 23255846 | solution.py:157
  350.3 3.0 select_exponential_fusion
  (218 shorter events, 111.2 us)
Async XLA Ops:
  7.2 130.0 %copy-start = (bf16[256,4096]{1,0:T(8,128)(2,1)S(1)}, bf16[256,4096]{1,0:T(8,128)(2,1)}, u32[]{:S(2)}) copy-start(bf16[256,4096]{1,0:T(8,128)(2,1)} %param.17) | copy-start | bytes 6291460
  7.2 4.5 %copy-start.9 = (bf16[256,2,4,128]{3,2,1,0:T(4,128)(2,1)S(1)}, bf16[256,2,4,128]{3,2,1,0:T(4,128)(2,1)}, u32[]{:S(2)}) copy-start(bf16[256,2,4,128]{3,2,1,0:T(4,128)(2,1)} %param.21) | copy-start | bytes 1572868
  7.2 4.7 %copy-start.5 = (bf16[256,4,128]{2,1,0:T(4,128)(2,1)S(1)}, bf16[256,4,128]{2,1,0:T(4,128)(2,1)}, u32[]{:S(2)}) copy-start(bf16[256,4,128]{2,1,0:T(4,128)(2,1)} %param.23) | copy-start | bytes 786436
  7.2 4.7 %copy-start.11 = (f32[128]{0:T(128)S(1)}, f32[128]{0:T(128)}, u32[]{:S(2)}) copy-start(f32[128]{0:T(128)} %param.25) | copy-start | bytes 1540
  7.2 55.4 %all-gather.5.cloned.1.call-start = ((), (), s32[]{:S(2)}) async-start(), calls=%async_computation.1 | async-start | bytes 2359296 | tf_op jit(solution)/shard_map/all_gather | solution.py:95
  9.1 5.9 %copy-start.6 = (bf16[256,4,128]{2,1,0:T(4,128)(2,1)S(1)}, bf16[256,4,128]{2,1,0:T(4,128)(2,1)}, u32[]{:S(2)}) copy-start(bf16[256,4,128]{2,1,0:T(4,128)(2,1)} %param.18) | copy-start | bytes 786436
  9.1 103.3 %all-gather.7.cloned.1.call-start = ((), (), s32[]{:S(2)}) async-start(), calls=%async_computation.2 | async-start | bytes 2359296 | tf_op jit(solution)/shard_map/all_gather | solution.py:96
  9.9 224.0 %all-gather.9.cloned.1.call-start = ((), (), s32[]{:S(2)}) async-start(), calls=%async_computation.3 | async-start | bytes 2359296 | tf_op jit(solution)/shard_map/all_gather | solution.py:127
  11.7 226.2 %all-gather.11.cloned.1.call-start = ((), (), s32[]{:S(2)}) async-start(), calls=%async_computation.4 | async-start | bytes 2359296 | tf_op jit(solution)/shard_map/all_gather | solution.py:128
  14.9 351.0 %reduce-scatter.2.cloned.1.call-start = ((), (), s32[]{:S(2)}) async-start(), calls=%async_computation.5 | async-start | bytes 4718592 | tf_op jit(solution)/shard_map/reduce_scatter | solution.py:163
  112.4 4.3 %copy-start.2 = (bf16[256,4,128]{2,0,1:T(8,128)(2,1)S(1)}, bf16[256,4,128]{2,0,1:T(8,128)(2,1)}, u32[]{:S(2)}) copy-start(bf16[256,4,128]{2,0,1:T(8,128)(2,1)} %get-tuple-element.774) | copy-start | bytes 786436
  112.4 4.3 %copy-start.10 = (f32[256,4,2]{0,2,1:T(2,128)S(1)}, f32[256,4,2]{0,2,1:T(2,128)}, u32[]{:S(2)}) copy-start(f32[256,4,2]{0,2,1:T(2,128)} %param.22) | copy-start | bytes 24580
  137.2 3.2 copy-start.4
  140.4 1.0 copy-start.7
  140.4 1.8 copy-start.8
  246.2 3.3 copy-start.3
  251.6 4.2 %copy-start.1 = (f32[4,2,256,256]{3,2,1,0:T(8,128)S(1)}, f32[4,2,256,256]{3,2,1,0:T(8,128)}, u32[]{:S(2)}) copy-start(f32[4,2,256,256]{3,2,1,0:T(8,128)} %select_exponential_fusion) | copy-start | bytes 6291460 | tf_op jit(solution)/shard_map/while/body/eval_jaxpr/cond
  261.1 3.3 copy-start.3
  266.4 4.2 %copy-start.1 = (f32[4,2,256,256]{3,2,1,0:T(8,128)S(1)}, f32[4,2,256,256]{3,2,1,0:T(8,128)}, u32[]{:S(2)}) copy-start(f32[4,2,256,256]{3,2,1,0:T(8,128)} %select_exponential_fusion) | copy-start | bytes 6291460 | tf_op jit(solution)/shard_map/while/body/eval_jaxpr/cond
  276.0 3.3 copy-start.3
  281.3 4.2 %copy-start.1 = (f32[4,2,256,256]{3,2,1,0:T(8,128)S(1)}, f32[4,2,256,256]{3,2,1,0:T(8,128)}, u32[]{:S(2)}) copy-start(f32[4,2,256,256]{3,2,1,0:T(8,128)} %select_exponential_fusion) | copy-start | bytes 6291460 | tf_op jit(solution)/shard_map/while/body/eval_jaxpr/cond
  290.8 3.3 copy-start.3
  296.1 4.2 %copy-start.1 = (f32[4,2,256,256]{3,2,1,0:T(8,128)S(1)}, f32[4,2,256,256]{3,2,1,0:T(8,128)}, u32[]{:S(2)}) copy-start(f32[4,2,256,256]{3,2,1,0:T(8,128)} %select_exponential_fusion) | copy-start | bytes 6291460 | tf_op jit(solution)/shard_map/while/body/eval_jaxpr/cond
  305.6 3.3 copy-start.3
  311.0 4.2 %copy-start.1 = (f32[4,2,256,256]{3,2,1,0:T(8,128)S(1)}, f32[4,2,256,256]{3,2,1,0:T(8,128)}, u32[]{:S(2)}) copy-start(f32[4,2,256,256]{3,2,1,0:T(8,128)} %select_exponential_fusion) | copy-start | bytes 6291460 | tf_op jit(solution)/shard_map/while/body/eval_jaxpr/cond
  320.4 3.3 copy-start.3
  325.8 4.2 %copy-start.1 = (f32[4,2,256,256]{3,2,1,0:T(8,128)S(1)}, f32[4,2,256,256]{3,2,1,0:T(8,128)}, u32[]{:S(2)}) copy-start(f32[4,2,256,256]{3,2,1,0:T(8,128)} %select_exponential_fusion) | copy-start | bytes 6291460 | tf_op jit(solution)/shard_map/while/body/eval_jaxpr/cond
  335.2 3.3 copy-start.3
  340.6 4.2 %copy-start.1 = (f32[4,2,256,256]{3,2,1,0:T(8,128)S(1)}, f32[4,2,256,256]{3,2,1,0:T(8,128)}, u32[]{:S(2)}) copy-start(f32[4,2,256,256]{3,2,1,0:T(8,128)} %select_exponential_fusion) | copy-start | bytes 6291460 | tf_op jit(solution)/shard_map/while/body/eval_jaxpr/cond
  350.0 3.3 copy-start.3
  355.4 4.2 %copy-start.1 = (f32[4,2,256,256]{3,2,1,0:T(8,128)S(1)}, f32[4,2,256,256]{3,2,1,0:T(8,128)}, u32[]{:S(2)}) copy-start(f32[4,2,256,256]{3,2,1,0:T(8,128)} %select_exponential_fusion) | copy-start | bytes 6291460 | tf_op jit(solution)/shard_map/while/body/eval_jaxpr/cond
Sparse Core Ops, SparseCore 0:
  10.8 51.7 all-gather.4
  64.7 47.6 all-gather.6
  114.6 47.7 all-gather.8
  164.4 47.3 all-gather.10
  215.3 88.2 reduce-scatter.1
where the time goes:
time: 377 us; the launch traced here: 375 us
  waiting for transfers between devices  93.3 us (25%)
  blocking collectives  90.8 us (24%)
  matrix products  78.8 us (21%)
  local copies, waits for them, and re-layouts  58.8 us (16%)
  other arithmetic  27.1 us (7%)
  between operations  13.9 us (4%)
  loops' own time  11.7 us (3%)
    all_gather x1, blocking collectives, body(): all_stats = lax.all_gather(row_stats, 'sp', axis=0, tiled=True)  90.8 us
    all_gather x1, waiting for transfers between devices, body(): key_piece = lax.all_gather(key_heads, 'sp', axis=0, tiled=True)  46.7 us
    all_gather x1, waiting for transfers between devices, body(): value_piece = lax.all_gather(value_heads, 'sp', axis=0, tiled=True)  45.8 us
    dot_general x8, matrix products, block_grads(): jnp.einsum('qhmd,khmd->hmqk', query_split, key_split, preferred_element_t...  24.2 us
    dynamic_slice x25, local copies, waits for them, and re-layouts, body(): result, _ = lax.scan(visit, local_zero, blocks)  24 us
    unnamed x30, local copies, waits for them, and re-layouts  23.9 us
    dot_general x8, matrix products, block_grads(): jnp.einsum('hqk,qhe->khe', diff_weights, grad_blk, preferred_element_type...  19 us
    dot_general x8, matrix products, block_grads(): jnp.einsum('hmqk,qhmd->khmd', score_grad, query_split, preferred_element_...  18.2 us
  transfers between devices with their start and end apart: 5, of which 2 were waited for; matrix products, arithmetic and copies ran while one was open for 43% of the time, Pallas kernels for 0%

commit v1 on v0

--- a/solution.py
+++ b/solution.py
@@ -92,8 +92,11 @@
     local_zero = jnp.zeros((rows_dev, head_count, width), jnp.float32)
     row_stats = jnp.concatenate([log_sums, row_terms], axis=-1)
     all_stats = lax.all_gather(row_stats, "sp", axis=0, tiled=True)
-    key_piece = lax.all_gather(key_heads, "sp", axis=0, tiled=True)
-    value_piece = lax.all_gather(value_heads, "sp", axis=0, tiled=True)
+    key_piece, value_piece = jnp.split(
+        lax.all_gather(jnp.concatenate([key_heads, value_heads], axis=1), "sp", axis=0, tiled=True),
+        [key_heads.shape[1]],
+        axis=1,
+    )
     pieces = key_piece.shape[0] // rows_dev
     blocks = (
         key_piece.reshape(pieces, rows_dev, head_count, width),

time: 377 us -> 362 us (0.960)
  waiting for transfers between devices: 93.3 us -> 69.8 us
  local copies, waits for them, and re-layouts: 58.8 us -> 65.5 us
    all_gather x2 -> x1, waiting for transfers between devices: 92.5 us -> 69.7 us  [body(): lax.all_gather(jnp.concatenate([key_heads, value_heads], axis=1), 'sp', a...]
    split x0 -> x1, local copies, waits for them, and re-layouts: none -> 4.5 us  [body(): jnp.split(lax.all_gather(jnp.concatenate([key_heads, value_heads], axis=1...]
    unnamed x30 -> x27, local copies, waits for them, and re-layouts: 23.9 us -> 24.8 us
  transfers between devices with their start and end apart: 5 -> 4, of which waited for: 2 -> 1; matrix products, arithmetic and copies ran while one was open for 43% -> 46% of each run, Pallas kernels for 0% -> 0%
where the time goes in v1:
time: 362 us; the launch traced here: 359 us
  blocking collectives  93.3 us (26%)
  matrix products  77.6 us (21%)
  waiting for transfers between devices  69.8 us (19%)
  local copies, waits for them, and re-layouts  65.5 us (18%)
  other arithmetic  27.9 us (8%)
  between operations  13.9 us (4%)
  loops' own time  11.3 us (3%)
    all_gather x1, blocking collectives, body(): all_stats = lax.all_gather(row_stats, 'sp', axis=0, tiled=True)  93.3 us
    all_gather x1, waiting for transfers between devices, body(): lax.all_gather(jnp.concatenate([key_heads, value_heads], axis=1), 'sp', a...  69.7 us
    unnamed x27, local copies, waits for them, and re-layouts  24.8 us
    dynamic_slice x25, local copies, waits for them, and re-layouts, body(): result, _ = lax.scan(visit, local_zero, blocks)  24.2 us
    dot_general x8, matrix products, block_grads(): jnp.einsum('qhmd,khmd->hmqk', query_split, key_split, preferred_element_t...  23.8 us
    dot_general x8, matrix products, block_grads(): jnp.einsum('hqk,qhe->khe', diff_weights, grad_blk, preferred_element_type...  19 us
    dot_general x8, matrix products, block_grads(): jnp.einsum('hmqk,qhmd->khmd', score_grad, query_split, preferred_element_...  18.1 us
    add x8, other arithmetic, accumulate(): return (key_acc + key_part, value_acc + value_part)  15.1 us
  transfers between devices with their start and end apart: 4, of which 1 were waited for; matrix products, arithmetic and copies ran while one was open for 46% of the time, Pallas kernels for 0%

profile of v1, /device:TPU:0, one launch (start us, length us, event | category | flops | bytes accessed | tf_op | source)
XLA Modules:
  0.0 359.4 jit_solution(10997214078482335960)
XLA Ops:
  16.6 69.7 %all-gather.4.cloned.1.call-done = bf16[2048,8,128]{2,0,1:T(8,128)(2,1)} async-done(((bf16[256,8,128]{2,0,1:T(8,128)(2,1)}), bf16[2048,8,128]{2,0,1:T(8,128)(2,1)}) %all-gather.4.cloned.1.call-update) | async-done | bytes 4194320 | tf_op jit(solution)/shard_map/all_gather | solution.py:96
  86.3 4.5 %fusion.43 = (bf16[2048,4,128]{2,0,1:T(8,128)(2,1)}, bf16[2048,4,128]{2,0,1:T(8,128)(2,1)}) fusion(bf16[2048,8,128]{2,0,1:T(8,128)(2,1)} %all-gather.4.cloned.1.call-done), kind=kLoop, calls=%fused_computation.81 | loop fusion | bytes 8388608 | tf_op jit(solution)/shard_map/split | solution.py:95
  90.8 4.0 %copy.34 = bf16[8,256,4,128]{1,3,2,0:T(8,128)(2,1)} copy(bf16[8,256,4,128]{3,1,0,2:T(8,128)(2,1)} %bitcast.119) | data formatting | bytes 4194304
  94.8 4.6 %copy.36 = bf16[8,256,4,128]{3,2,1,0:T(4,128)(2,1)} copy(bf16[8,256,4,128]{3,1,0,2:T(8,128)(2,1)} %bitcast.118) | data formatting | bytes 4194304
  100.2 19.5 %while.30 = (s32[]{:T(128)}, f32[256,4,128]{0,2,1:T(8,128)}, s32[8]{0:T(128)S(1)}, s32[]{:T(128)}, f32[4]{0:T(128)}, /*index=5*/bf16[8,256,4,128]{1,3,2,0:T(8,12...) while((s32[]{:T(128)}, f32[256,4,128]{0,2,1:T(8,128)}, ...), condition=%wide.region_7.8_spmd.clone, body=%wide.region_4.7_spmd.clone.sunk | while | flops 205324800 | bytes 6445503 | solution.py:128
  101.5 9.3 %conditional.7 = (f32[256,4,128]{0,2,1:T(8,128)}) conditional(s32[]{:T(128)} %convert_element_type.109, f32[256,4,128]{0,2,1:T(8,128)} %get-tuple-element.755, (f32[4]{0:T(128)}, s32[]{:T(128)}, s32[]{:T(128)}, bf16[8,256,4,128]{1,3,2,0:T(8,128)(2,1)}, s32[]{:T(128)}, /*index=5*/bf16[256,4,128]{0,2,1:T(8,128)(2,1)}, f32[256,4,2]{0,2,1:T(2,128)S(1)}, ...), branch_computations={%region_5.5_spmd, %region_6.6_spmd} | conditional | flops 205324800 | bytes 6444204 | solution.py:126
  105.5 3.2 fusion.9
  121.1 3.2 fusion.38
  126.1 93.3 %all_gather.14 = f32[2048,4,4]{0,2,1:T(4,128)S(1)} all-gather(f32[256,4,4]{0,2,1:T(4,128)S(1)} %pad_maximum_fusion.1), channel_id=1, replica_groups=mesh['sp'=8,'tp'=4] {'sp'}, dimensions={0}, use_global_device_ids=true | all-gather | bytes 147456 | tf_op jit(solution)/shard_map/all_gather | solution.py:94
  219.5 4.0 %copy.41 = bf16[8,256,4,128]{1,3,2,0:T(8,128)(2,1)} copy(bf16[8,256,4,128]{3,1,0,2:T(8,128)(2,1)} %bitcast.121) | data formatting | bytes 4194304
  223.4 3.2 copy.43
  228.8 117.8 %while.31 = (s32[]{:T(128)}, f32[256,4,128]{0,2,1:T(8,128)}, f32[256,4,128]{2,0,1:T(8,128)}, s32[8]{0:T(128)}, s32[]{:T(128)}, /*index=5*/f32[4]{0:T(128)}, bf16...) while((s32[]{:T(128)}, f32[256,4,128]{0,2,1:T(8,128)}, ...), condition=%wide.region_11.12_spmd.clone.clone, body=%wide.region_8.11_spmd.clone.clone.sunk | while | flops 273351168 | bytes 23257172 | solution.py:162
  230.7 12.8 %conditional.8 = ((f32[256,4,128]{0,2,1:T(8,128)}, f32[256,4,128]{2,0,1:T(8,128)})) conditional(s32[]{:T(128)} %convert_element_type.110, (f32[256,4,128]{0,2,1:T(8,128)}, f32[256,4,128]{2,0,1:T(8,128)}) %tuple.99, (f32[4]{0:T(128)}, s32[]{:T(128)}, s32[]{:T(128)}, bf16[8,256,4,128]{1,3,2,0:T(8,128)(2,1)}, s32[]{:T(128)}, ...), branch_computations={%region_9.9_spmd, %region_10.10_spmd} | conditional | flops 273351168 | bytes 23255846 | solution.py:160
  232.0 3.0 select_exponential_fusion
  241.2 2.4 fusion.21
  245.5 12.8 %conditional.8 = ((f32[256,4,128]{0,2,1:T(8,128)}, f32[256,4,128]{2,0,1:T(8,128)})) conditional(s32[]{:T(128)} %convert_element_type.110, (f32[256,4,128]{0,2,1:T(8,128)}, f32[256,4,128]{2,0,1:T(8,128)}) %tuple.99, (f32[4]{0:T(128)}, s32[]{:T(128)}, s32[]{:T(128)}, bf16[8,256,4,128]{1,3,2,0:T(8,128)(2,1)}, s32[]{:T(128)}, ...), branch_computations={%region_9.9_spmd, %region_10.10_spmd} | conditional | flops 273351168 | bytes 23255846 | solution.py:160
  246.7 3.0 select_exponential_fusion
  255.9 2.4 fusion.21
  260.2 12.8 %conditional.8 = ((f32[256,4,128]{0,2,1:T(8,128)}, f32[256,4,128]{2,0,1:T(8,128)})) conditional(s32[]{:T(128)} %convert_element_type.110, (f32[256,4,128]{0,2,1:T(8,128)}, f32[256,4,128]{2,0,1:T(8,128)}) %tuple.99, (f32[4]{0:T(128)}, s32[]{:T(128)}, s32[]{:T(128)}, bf16[8,256,4,128]{1,3,2,0:T(8,128)(2,1)}, s32[]{:T(128)}, ...), branch_computations={%region_9.9_spmd, %region_10.10_spmd} | conditional | flops 273351168 | bytes 23255846 | solution.py:160
  261.4 3.0 select_exponential_fusion
  270.7 2.4 fusion.21
  274.9 12.8 %conditional.8 = ((f32[256,4,128]{0,2,1:T(8,128)}, f32[256,4,128]{2,0,1:T(8,128)})) conditional(s32[]{:T(128)} %convert_element_type.110, (f32[256,4,128]{0,2,1:T(8,128)}, f32[256,4,128]{2,0,1:T(8,128)}) %tuple.99, (f32[4]{0:T(128)}, s32[]{:T(128)}, s32[]{:T(128)}, bf16[8,256,4,128]{1,3,2,0:T(8,128)(2,1)}, s32[]{:T(128)}, ...), branch_computations={%region_9.9_spmd, %region_10.10_spmd} | conditional | flops 273351168 | bytes 23255846 | solution.py:160
  276.2 3.0 select_exponential_fusion
  289.7 12.8 %conditional.8 = ((f32[256,4,128]{0,2,1:T(8,128)}, f32[256,4,128]{2,0,1:T(8,128)})) conditional(s32[]{:T(128)} %convert_element_type.110, (f32[256,4,128]{0,2,1:T(8,128)}, f32[256,4,128]{2,0,1:T(8,128)}) %tuple.99, (f32[4]{0:T(128)}, s32[]{:T(128)}, s32[]{:T(128)}, bf16[8,256,4,128]{1,3,2,0:T(8,128)(2,1)}, s32[]{:T(128)}, ...), branch_computations={%region_9.9_spmd, %region_10.10_spmd} | conditional | flops 273351168 | bytes 23255846 | solution.py:160
  290.9 3.0 select_exponential_fusion
  300.1 2.4 fusion.21
  304.4 12.8 %conditional.8 = ((f32[256,4,128]{0,2,1:T(8,128)}, f32[256,4,128]{2,0,1:T(8,128)})) conditional(s32[]{:T(128)} %convert_element_type.110, (f32[256,4,128]{0,2,1:T(8,128)}, f32[256,4,128]{2,0,1:T(8,128)}) %tuple.99, (f32[4]{0:T(128)}, s32[]{:T(128)}, s32[]{:T(128)}, bf16[8,256,4,128]{1,3,2,0:T(8,128)(2,1)}, s32[]{:T(128)}, ...), branch_computations={%region_9.9_spmd, %region_10.10_spmd} | conditional | flops 273351168 | bytes 23255846 | solution.py:160
  305.6 3.0 select_exponential_fusion
  319.1 12.8 %conditional.8 = ((f32[256,4,128]{0,2,1:T(8,128)}, f32[256,4,128]{2,0,1:T(8,128)})) conditional(s32[]{:T(128)} %convert_element_type.110, (f32[256,4,128]{0,2,1:T(8,128)}, f32[256,4,128]{2,0,1:T(8,128)}) %tuple.99, (f32[4]{0:T(128)}, s32[]{:T(128)}, s32[]{:T(128)}, bf16[8,256,4,128]{1,3,2,0:T(8,128)(2,1)}, s32[]{:T(128)}, ...), branch_computations={%region_9.9_spmd, %region_10.10_spmd} | conditional | flops 273351168 | bytes 23255846 | solution.py:160
  320.3 3.0 select_exponential_fusion
  333.8 12.8 %conditional.8 = ((f32[256,4,128]{0,2,1:T(8,128)}, f32[256,4,128]{2,0,1:T(8,128)})) conditional(s32[]{:T(128)} %convert_element_type.110, (f32[256,4,128]{0,2,1:T(8,128)}, f32[256,4,128]{2,0,1:T(8,128)}) %tuple.99, (f32[4]{0:T(128)}, s32[]{:T(128)}, s32[]{:T(128)}, bf16[8,256,4,128]{1,3,2,0:T(8,128)(2,1)}, s32[]{:T(128)}, ...), branch_computations={%region_9.9_spmd, %region_10.10_spmd} | conditional | flops 273351168 | bytes 23255846 | solution.py:160
  335.0 3.0 select_exponential_fusion
  (215 shorter events, 111.3 us)
Async XLA Ops:
  7.2 113.9 %copy-start = (bf16[256,4096]{1,0:T(8,128)(2,1)S(1)}, bf16[256,4096]{1,0:T(8,128)(2,1)}, u32[]{:S(2)}) copy-start(bf16[256,4096]{1,0:T(8,128)(2,1)} %param.17) | copy-start | bytes 6291460
  7.2 3.2 copy-start.5
  7.2 4.0 %copy-start.7 = (bf16[256,2,4,128]{3,2,1,0:T(4,128)(2,1)S(1)}, bf16[256,2,4,128]{3,2,1,0:T(4,128)(2,1)}, u32[]{:S(2)}) copy-start(bf16[256,2,4,128]{3,2,1,0:T(4,128)(2,1)} %param.21) | copy-start | bytes 1572868
  7.2 79.1 %all-gather.4.cloned.1.call-start = ((), (), s32[]{:S(2)}) async-start(), calls=%async_computation.1 | async-start | bytes 4718592 | tf_op jit(solution)/shard_map/all_gather | solution.py:96
  8.4 3.0 copy-start.4
  8.4 3.0 copy-start.9
  10.3 209.1 %all-gather.6.cloned.1.call-start = ((), (), s32[]{:S(2)}) async-start(), calls=%async_computation.2 | async-start | bytes 2359296 | tf_op jit(solution)/shard_map/all_gather | solution.py:130
  11.2 212.3 %all-gather.8.cloned.1.call-start = ((), (), s32[]{:S(2)}) async-start(), calls=%async_computation.3 | async-start | bytes 2359296 | tf_op jit(solution)/shard_map/all_gather | solution.py:131
  14.4 336.2 %reduce-scatter.2.cloned.1.call-start = ((), (), s32[]{:S(2)}) async-start(), calls=%async_computation.4 | async-start | bytes 4718592 | tf_op jit(solution)/shard_map/reduce_scatter | solution.py:166
  94.8 5.5 %copy-start.8 = (f32[256,4,2]{0,2,1:T(2,128)S(1)}, f32[256,4,2]{0,2,1:T(2,128)}, u32[]{:S(2)}) copy-start(f32[256,4,2]{0,2,1:T(2,128)} %param.22) | copy-start | bytes 24580
  121.0 3.2 copy-start.3
  124.3 1.0 copy-start.6
  231.7 3.2 copy-start.2
  237.0 4.2 %copy-start.1 = (f32[4,2,256,256]{3,2,1,0:T(8,128)S(1)}, f32[4,2,256,256]{3,2,1,0:T(8,128)}, u32[]{:S(2)}) copy-start(f32[4,2,256,256]{3,2,1,0:T(8,128)} %select_exponential_fusion) | copy-start | bytes 6291460 | tf_op jit(solution)/shard_map/while/body/eval_jaxpr/cond
  246.5 3.2 copy-start.2
  251.8 4.2 %copy-start.1 = (f32[4,2,256,256]{3,2,1,0:T(8,128)S(1)}, f32[4,2,256,256]{3,2,1,0:T(8,128)}, u32[]{:S(2)}) copy-start(f32[4,2,256,256]{3,2,1,0:T(8,128)} %select_exponential_fusion) | copy-start | bytes 6291460 | tf_op jit(solution)/shard_map/while/body/eval_jaxpr/cond
  261.2 3.2 copy-start.2
  266.5 4.2 %copy-start.1 = (f32[4,2,256,256]{3,2,1,0:T(8,128)S(1)}, f32[4,2,256,256]{3,2,1,0:T(8,128)}, u32[]{:S(2)}) copy-start(f32[4,2,256,256]{3,2,1,0:T(8,128)} %select_exponential_fusion) | copy-start | bytes 6291460 | tf_op jit(solution)/shard_map/while/body/eval_jaxpr/cond
  275.9 3.2 copy-start.2
  281.2 4.2 %copy-start.1 = (f32[4,2,256,256]{3,2,1,0:T(8,128)S(1)}, f32[4,2,256,256]{3,2,1,0:T(8,128)}, u32[]{:S(2)}) copy-start(f32[4,2,256,256]{3,2,1,0:T(8,128)} %select_exponential_fusion) | copy-start | bytes 6291460 | tf_op jit(solution)/shard_map/while/body/eval_jaxpr/cond
  290.7 3.2 copy-start.2
  295.9 4.2 %copy-start.1 = (f32[4,2,256,256]{3,2,1,0:T(8,128)S(1)}, f32[4,2,256,256]{3,2,1,0:T(8,128)}, u32[]{:S(2)}) copy-start(f32[4,2,256,256]{3,2,1,0:T(8,128)} %select_exponential_fusion) | copy-start | bytes 6291460 | tf_op jit(solution)/shard_map/while/body/eval_jaxpr/cond
  305.4 3.2 copy-start.2
  310.7 4.2 %copy-start.1 = (f32[4,2,256,256]{3,2,1,0:T(8,128)S(1)}, f32[4,2,256,256]{3,2,1,0:T(8,128)}, u32[]{:S(2)}) copy-start(f32[4,2,256,256]{3,2,1,0:T(8,128)} %select_exponential_fusion) | copy-start | bytes 6291460 | tf_op jit(solution)/shard_map/while/body/eval_jaxpr/cond
  320.1 3.2 copy-start.2
  325.4 4.2 %copy-start.1 = (f32[4,2,256,256]{3,2,1,0:T(8,128)S(1)}, f32[4,2,256,256]{3,2,1,0:T(8,128)}, u32[]{:S(2)}) copy-start(f32[4,2,256,256]{3,2,1,0:T(8,128)} %select_exponential_fusion) | copy-start | bytes 6291460 | tf_op jit(solution)/shard_map/while/body/eval_jaxpr/cond
  334.8 3.2 copy-start.2
  340.1 4.2 %copy-start.1 = (f32[4,2,256,256]{3,2,1,0:T(8,128)S(1)}, f32[4,2,256,256]{3,2,1,0:T(8,128)}, u32[]{:S(2)}) copy-start(f32[4,2,256,256]{3,2,1,0:T(8,128)} %select_exponential_fusion) | copy-start | bytes 6291460 | tf_op jit(solution)/shard_map/while/body/eval_jaxpr/cond
Sparse Core Ops, SparseCore 0:
  10.8 75.4 all-gather.3
  88.5 47.5 all-gather.5
  138.8 47.8 all-gather.7
  190.3 87.9 reduce-scatter.1
